TPU v7x, 32 devices: a whole 2x2x4 slice. The times are simulated.
32 devices in a mesh: sp: 8 (over z, core), tp: 4 (over y, x).
Axes of the slice: x: 2, y: 2, z: 4, core: 2. Of those that a mesh axis runs over, the one named last changes fastest.
Arguments:
- cell_query_heads: bfloat16 [1024, 2048], P('sp', 'tp'), may hold values from -6 to 6
- cell_key_heads: bfloat16 [1024, 2048], P('sp', 'tp'), may hold values from -6 to 6
- cell_value_heads: bfloat16 [1024, 2048], P('sp', 'tp'), may hold values from -6 to 6
- output_gate_logits: bfloat16 [1024, 2048], P('sp', 'tp'), may hold values from -6 to 6
- input_gate_log: float32 [1024, 16], P('sp', 'tp'), may hold values from -7 to 310
- forget_gate_logits: float32 [1024, 16], P('sp', 'tp'), may hold values from 1 to 14
- extra_log_decay: float32 [1024, 16], P('sp', 'tp'), may hold values from -1 to 0
- documents: int32 [1024], P('sp'), may hold values from 0 to 7, never falling along the last dimension, each value on 1 to 256 neighbouring positions
- head_norm_gain: float32 [2048], P('tp'), may hold values from 0.1 to 1.9
- stream: bfloat16 [1024, 4096], P('sp', 'tp'), may hold values from -6 to 6
- output_weight: bfloat16 [2048, 4096], P(None, 'tp'), may hold values from -0.125 to 0.125
- expert_norm_gain: bfloat16 [4096], P('tp'), may hold values from 0.099609375 to 1.8984375
- expert_choice_index: int32 [1024, 2], P('sp'), may hold values from 0 to 7, all different within a row; in each aligned block of 128 rows (0 to 127, 128 to 255, ...) at most 64 rows name the same one
- routing_weight: float32 [1024, 2], P('sp'), may hold values from 0.2 to 1
- gate_weight: bfloat16 [8, 4096, 2048], P('sp', None, 'tp'), may hold values from -0.09375 to 0.09375
- up_weight: bfloat16 [8, 4096, 2048], P('sp', None, 'tp'), may hold values from -0.09375 to 0.09375
- down_weight: bfloat16 [8, 2048, 4096], P('sp', None, 'tp'), may hold values from -0.125 to 0.125
Outputs:
- output: bfloat16 [1024, 4096], P('sp', 'tp')
Inputs may be any that keep to these rules, and one draw needn't show every extreme that they name: `expert_choice_index`: in the rows of one index of sp no expert is named more than 64 times, a bound that some block reaches. `documents`: never falling; each document 1 to 256 positions, one exactly 256.
All inputs are finite; a program needn't handle non-finite values.
Results may differ from a plain program's by a relative error of at most 0.01.
Values may be sent and summed in bfloat16 or wider, within the bound.
A program may use at most 64 MiB of HBM per device.

v0:
```python
import jax
import jax.numpy as jnp
from jax import lax
from jax.sharding import PartitionSpec as P

D = 4096
HD = 128
TOPK = 2
EPSILON = 1e-06
LOW_LOG = -1e30
HIGHEST = lax.Precision.HIGHEST


def prefix_2(part, axis, combine, identity):
    place = lax.axis_index(axis)
    gathered = jax.tree.map(lambda a: lax.all_gather(a, axis), part)
    state = jax.tree.map(lambda a, e: jnp.zeros_like(a) + jnp.asarray(e, a.dtype), part, identity)

    def one(turn, state):
        return combine(
            state, jax.tree.map(lambda a: lax.dynamic_index_in_dim(a, turn, 0, False), gathered)
        )

    return lax.fori_loop(0, place, one, state)


def empty_summary(heads, width):
    return (
        jnp.zeros((heads, width, width), jnp.float32),
        jnp.zeros((heads, width), jnp.float32),
        jnp.full((heads,), LOW_LOG, jnp.float32),
        jnp.zeros((heads,), jnp.float32),
        jnp.zeros((), jnp.int32),
        jnp.full((), -1, jnp.int32),
        jnp.full((), -1, jnp.int32),
    )


def block_summary(key_f, value_f, decay_logarithm, input_gate_log, documents, first_global):
    length = documents.shape[0]
    positions = jnp.arange(length, dtype=jnp.int32)
    cumulative = jnp.cumsum(decay_logarithm, axis=0)
    total_log = cumulative[-1]
    prior_log = cumulative - decay_logarithm
    starts = jnp.concatenate([jnp.reshape(first_global, (1,)), documents[1:] != documents[:-1]])
    inside = jnp.any(starts)
    last_start = jnp.max(jnp.where(starts, positions, -1))
    base_log = jnp.sum(jnp.where((positions == last_start)[:, None], prior_log, 0.0), axis=0)
    in_last = (documents == documents[-1])[:, None]
    weight_log = total_log[None, :] - cumulative + input_gate_log
    peak_log = jnp.max(jnp.where(in_last, weight_log, LOW_LOG), axis=0)
    peak_log = jnp.where(inside, jnp.maximum(peak_log, total_log - base_log), peak_log)
    weights = jnp.where(in_last, jnp.exp(jnp.minimum(weight_log - peak_log[None, :], 0.0)), 0.0)
    matrix = jnp.einsum("lhd,lhe->hde", weights[:, :, None] * key_f, value_f, precision=HIGHEST)
    normer = jnp.sum(weights[:, :, None] * key_f, axis=0)
    return (
        matrix,
        normer,
        peak_log,
        total_log,
        inside.astype(jnp.int32),
        documents[0],
        documents[-1],
    )


def combine(early, late):
    broken = late[5] != early[6]
    carry_matrix = jnp.where(broken, 0.0, early[0])
    carry_normer = jnp.where(broken, 0.0, early[1])
    carry_peak = jnp.where(broken, 0.0, early[2])
    joined = jnp.maximum(late[3] + carry_peak, late[2])
    older = jnp.exp(late[3] + carry_peak - joined)
    newer = jnp.exp(late[2] - joined)
    resets = late[4] > 0
    matrix = jnp.where(
        resets, late[0], older[:, None, None] * carry_matrix + newer[:, None, None] * late[0]
    )
    normer = jnp.where(resets, late[1], older[:, None] * carry_normer + newer[:, None] * late[1])
    peak_log = jnp.where(resets, late[2], joined)
    flags = jnp.maximum(jnp.maximum(early[4], late[4]), broken.astype(jnp.int32))
    merged = (matrix, normer, peak_log, early[3] + late[3], flags, early[5], late[6])
    early_empty = early[6] < 0
    late_empty = late[6] < 0
    return tuple(
        (
            jnp.where(early_empty, second, jnp.where(late_empty, first_item, joint))
            for first_item, second, joint in zip(early, late, merged)
        )
    )


def block_output(query_f, key_f, value_f, decay_logarithm, input_gate_log, documents, prefix):
    prev_matrix, prev_normer, prev_peak, _, _, _, prev_last = prefix
    length = documents.shape[0]
    positions = jnp.arange(length, dtype=jnp.int32)
    cumulative = jnp.cumsum(decay_logarithm, axis=0)
    prior_log = cumulative - decay_logarithm
    before = jnp.concatenate([jnp.reshape(prev_last, (1,)), documents[:-1]])
    starts = documents != before
    last_start = lax.cummax(jnp.where(starts, positions, -1), axis=0)
    started = last_start >= 0
    picker = (positions[None, :] == last_start[:, None]).astype(jnp.float32)
    base_log = jnp.dot(picker, prior_log, precision=HIGHEST)
    carry_log = (cumulative + jnp.where(started[:, None], -base_log, prev_peak[None, :])).T
    same_doc = (documents[:, None] == documents[None, :]) & (
        positions[:, None] >= positions[None, :]
    )
    cum_heads = cumulative.T
    pair_log = cum_heads[:, :, None] - cum_heads[:, None, :] + input_gate_log.T[:, None, :]
    pair_log = jnp.where(same_doc[None], pair_log, LOW_LOG)
    peak_log = jnp.maximum(carry_log, jnp.max(pair_log, axis=-1))
    weights = jnp.exp(pair_log - peak_log[:, :, None])
    scores = jnp.einsum("lhd,shd->hls", query_f, key_f, precision=HIGHEST) * weights
    carry_scale = jnp.where(started[None, :], 0.0, jnp.exp(carry_log - peak_log))
    numer = jnp.einsum("hls,she->hle", scores, value_f, precision=HIGHEST)
    numer = numer + carry_scale[:, :, None] * jnp.einsum(
        "lhd,hde->hle", query_f, prev_matrix, precision=HIGHEST
    )
    denom = jnp.sum(scores, axis=-1) + carry_scale * jnp.einsum(
        "lhd,hd->hl", query_f, prev_normer, precision=HIGHEST
    )
    cell_vals = numer / jnp.maximum(jnp.abs(denom), jnp.exp(-peak_log))[:, :, None]
    return jnp.transpose(cell_vals, (1, 0, 2))


def finish_cell(cell_vals, output_gate_logits, head_norm_gain):
    length, heads, width = cell_vals.shape
    gated_cell = (
        jax.nn.sigmoid(output_gate_logits.astype(jnp.float32)).reshape(length, heads, width)
        * cell_vals
    )
    scaled = gated_cell * lax.rsqrt(
        jnp.mean(gated_cell * gated_cell, axis=-1, keepdims=True) + EPSILON
    )
    scaled = scaled * head_norm_gain.reshape(heads, width)
    return scaled.reshape(length, heads * width).astype(jnp.bfloat16)


def expert_work(row_block, gate_weight, up_weight, down_weight):
    gate_act = jnp.einsum(
        "sqid,qdf->sqif", row_block, gate_weight, preferred_element_type=jnp.float32
    )
    upward = jnp.einsum("sqid,qdf->sqif", row_block, up_weight, preferred_element_type=jnp.float32)
    hidden = (jax.nn.silu(gate_act) * upward).astype(jnp.bfloat16)
    result = jnp.einsum(
        "sqif,qfe->sqie",
        lax.all_gather(hidden, "tp", axis=3, tiled=True),
        down_weight,
        preferred_element_type=jnp.float32,
    )
    return result.astype(jnp.bfloat16)


def per_device(
    cell_query_heads,
    cell_key_heads,
    cell_value_heads,
    output_gate_logits,
    input_gate_log,
    forget_gate_logits,
    extra_log_decay,
    documents,
    head_norm_gain,
    stream,
    output_weight,
    expert_norm_gain,
    expert_choice_index,
    routing_weight,
    gate_weight,
    up_weight,
    down_weight,
):
    tokens = documents.shape[0]
    local_heads = input_gate_log.shape[1]
    shaped = (tokens, local_heads, HD)
    query_f = cell_query_heads.astype(jnp.float32).reshape(shaped)
    key_f = cell_key_heads.astype(jnp.float32).reshape(shaped) * HD ** (-0.5)
    value_f = cell_value_heads.astype(jnp.float32).reshape(shaped)
    decay_logarithm = jax.nn.log_sigmoid(forget_gate_logits) + extra_log_decay
    first_global = lax.axis_index("sp") == 0
    summary = block_summary(
        key_f, value_f, decay_logarithm, input_gate_log, documents, first_global
    )
    prefix = prefix_2(summary, "sp", combine, empty_summary(local_heads, HD))
    cell_vals = block_output(
        query_f, key_f, value_f, decay_logarithm, input_gate_log, documents, prefix
    )
    memory_cell_output = finish_cell(cell_vals, output_gate_logits, head_norm_gain)
    projected = jnp.dot(
        lax.all_gather(memory_cell_output, "tp", axis=1, tiled=True),
        output_weight,
        preferred_element_type=jnp.float32,
    )
    resid = (stream.astype(jnp.float32) + projected).astype(jnp.bfloat16)
    groups = lax.axis_size("sp")
    experts_all = groups * gate_weight.shape[0]
    capacity = 2 * tokens * TOPK // experts_all
    flat_ids = expert_choice_index.reshape(-1)
    onehot = (flat_ids[:, None] == jnp.arange(experts_all, dtype=jnp.int32)[None, :]).astype(
        jnp.int32
    )
    rank_in = jnp.sum((jnp.cumsum(onehot, axis=0) - onehot) * onehot, axis=1)
    slot_of = (flat_ids * capacity + rank_in).reshape(tokens, TOPK)
    slot_index = jnp.arange(experts_all * capacity, dtype=jnp.int32)
    chooser = jnp.any(slot_index[:, None, None] == slot_of[None, :, :], axis=2).astype(jnp.bfloat16)
    bucket_shape = (groups, gate_weight.shape[0], capacity)
    rows_f = resid.astype(jnp.float32)
    squares = lax.psum(jnp.sum(rows_f * rows_f, axis=1), "tp")
    normed = rows_f * lax.rsqrt(squares[:, None] / D + EPSILON)
    normed = (normed * expert_norm_gain.astype(jnp.float32)[None, :]).astype(jnp.bfloat16)
    packed = jnp.dot(chooser, normed, preferred_element_type=jnp.float32).astype(jnp.bfloat16)
    packed = packed.reshape(bucket_shape + (normed.shape[1],))
    row_block = lax.all_gather(
        lax.all_to_all(packed, "sp", split_axis=0, concat_axis=0, tiled=True),
        "tp",
        axis=3,
        tiled=True,
    )
    served = expert_work(row_block, gate_weight, up_weight, down_weight)
    returned = lax.all_to_all(served, "sp", split_axis=0, concat_axis=0, tiled=True).reshape(
        -1, served.shape[3]
    )
    mixed = resid.astype(jnp.float32)
    for ordinal in range(TOPK):
        selector = (slot_of[:, ordinal][:, None] == slot_index[None, :]).astype(jnp.bfloat16)
        picked = jnp.dot(selector, returned, preferred_element_type=jnp.float32)
        mixed = mixed + routing_weight[:, ordinal : ordinal + 1] * picked
    return mixed.astype(jnp.bfloat16)


def solution(mesh):
    placed = (
        P("sp", "tp"),
        P("sp", "tp"),
        P("sp", "tp"),
        P("sp", "tp"),
        P("sp", "tp"),
        P("sp", "tp"),
        P("sp", "tp"),
        P("sp"),
        P("tp"),
        P("sp", "tp"),
        P(None, "tp"),
        P("tp"),
        P("sp", None),
        P("sp", None),
        P("sp", None, "tp"),
        P("sp", None, "tp"),
        P("sp", None, "tp"),
    )
    return jax.shard_map(
        per_device, mesh=mesh, in_specs=placed, out_specs=P("sp", "tp"), check_vma=False
    )
```

profile of v0, /device:TPU:0, one launch (start us, length us, event | category | flops | bytes accessed | tf_op | source)
XLA Modules:
  0.0 303.4 jit_solution(6847889655338509931)
XLA Ops:
  6.6 0.8 fusion.74
  7.5 0.2 reduce_window_sum.27
  7.7 1.5 fusion.81
  9.2 1.3 dynamic-slice
  10.5 2.0 slice_dynamic-update-slice_fusion
  12.5 1.3 broadcast_compare_fusion.1
  13.8 0.7 fusion.78
  14.5 0.6 iota_compare_fusion.10
  15.7 0.9 select_reduce_fusion
  16.7 0.8 select_multiply_fusion
  17.4 1.0 copy.177
  18.5 1.0 copy.183
  19.5 1.1 fusion.61
  20.7 0.7 dynamic-update-slice.1
  21.4 1.4 slice_dynamic-update-slice_fusion.1
  22.8 10.6 %all-reduce.3 = (s32[8]{0:T(128)S(1)}, s32[8]{0:T(128)S(1)}, s32[8]{0:T(128)S(1)}) all-reduce(s32[8]{0:T(128)S(1)} %slice_dynamic-update-slice_fusion.1, s32[8]{0:T(128)S(1)} %dynamic-update-slice.1, s32[8]{0:T(128)S(1)} %get-tuple-element.244), channel_id=1, replica_groups=mesh['sp'=8,'tp'=4] {'sp'}, use_global_device_ids=true, to_apply=%add | all-reduce | flops 24 | bytes 192
  33.4 0.8 copy.162
  34.2 0.1 eq.129
  34.4 0.1 eq.125
  34.7 1.0 copy.176
  35.7 1.0 add_divide_fusion
  36.8 0.6 reduce-window.18
  37.4 0.2 slice_reduce_fusion
  37.8 0.1 reduce_sum.67
  38.0 9.5 %all-gather.2 = f32[8,1,4]{2,1,0:T(1,128)S(1)} all-gather(f32[1,1,4]{2,1,0:T(1,128)S(1)} %bitcast.270), channel_id=1, replica_groups=mesh['sp'=8,'tp'=4] {'sp'}, dimensions={0}, use_global_device_ids=true | all-gather | bytes 144 | tf_op jit(solution)/shard_map/all_gather | solution.py:16
  47.5 10.1 %all-gather.1 = f32[8,1,4]{2,1,0:T(1,128)S(1)} all-gather(f32[1,1,4]{2,1,0:T(1,128)S(1)} %get-tuple-element.235), channel_id=1, replica_groups=mesh['sp'=8,'tp'=4] {'sp'}, dimensions={0}, use_global_device_ids=true | all-gather | bytes 144 | tf_op jit(solution)/shard_map/all_gather | solution.py:16
  57.7 12.8 %all_gather.53 = f32[8,4,128]{2,1,0:T(4,128)S(1)} all-gather(f32[1,4,128]{2,1,0:T(4,128)S(1)} %bitcast.267), channel_id=1, replica_groups=mesh['sp'=8,'tp'=4] {'sp'}, dimensions={0}, use_global_device_ids=true | all-gather | bytes 18432 | tf_op jit(solution)/shard_map/all_gather | solution.py:16
  70.6 0.2 fusion.63
  71.1 0.2 reduce-window.14
  71.4 0.2 add_maximum_fusion
  71.6 0.4 fusion.82
  72.0 0.3 convolution_bitcast_fusion.1
  72.3 0.2 fusion.83
  72.5 0.4 multiply_reduce_fusion.1
  73.1 9.6 %all_gather.54 = bf16[128,2048]{0,1:T(8,128)(2,1)S(1)} all-gather(bf16[128,512]{0,1:T(8,128)(2,1)S(1)} %bitcast.254), channel_id=1, replica_groups=mesh['sp'=8,'tp'=4] {'tp'}, dimensions={1}, use_global_device_ids=true | all-gather | bytes 655360 | tf_op jit(solution)/shard_map/all_gather | solution.py:191
  82.7 3.0 multiply_reduce_fusion
  85.8 9.0 %psum.7 = f32[128]{0:T(128)S(1)} all-reduce(f32[128]{0:T(128)S(1)} %get-tuple-element.252), channel_id=1, replica_groups=mesh['sp'=8,'tp'=4] {'tp'}, use_global_device_ids=true, to_apply=%region_17.18 | all-reduce | flops 128 | bytes 1024 | tf_op jit(solution)/shard_map/psum | solution.py:209
  94.7 0.5 convolution_convert_fusion
  95.3 67.8 %all_to_all.10 = bf16[8,1,64,1024]{3,2,1,0:T(8,128)(2,1)} all-to-all(bf16[8,1,64,1024]{3,2,1,0:T(8,128)(2,1)S(1)} %bitcast.247), channel_id=1, replica_groups=mesh['sp'=8,'tp'=4] {'sp'}, dimensions={0} | all-to-all | bytes 2097152 | tf_op jit(solution)/shard_map/all_to_all | solution.py:215
  163.1 50.6 %all-gather.7.cloned.1.call-done = bf16[8,1,64,4096]{3,2,0,1:T(8,128)(2,1)} async-done(((bf16[8,1,64,1024]{3,2,0,1:T(8,128)(2,1)}), bf16[8,1,64,4096]{3,2,0,1:T(8,128)(2,1)}) %all-gather.7.cloned.1.call-update) | async-done | bytes 4194320 | tf_op jit(solution)/shard_map/all_gather | solution.py:214
  213.7 5.9 %fusion.26 = f32[8,1,64,512]{3,2,0,1:T(8,128)S(1)} fusion(bf16[1,4096,512]{2,1,0:T(8,128)(2,1)} %param.33, bf16[8,1,64,4096]{3,2,0,1:T(8,128)(2,1)} %all-gather.7.cloned.1.call-done), kind=kOutput, calls=%fused_computation.33 | convolution fusion | flops 2147483648 | bytes 9437184 | tf_op jit(solution)/shard_map/sqid,qdf->sqif/dot_general | solution.py:141
  219.7 3.2 %fusion.41 = bf16[8,1,64,512]{3,2,0,1:T(8,128)(2,1)} fusion(bf16[1,4096,512]{2,1,0:T(8,128)(2,1)S(1)} %copy-done.8, bf16[8,1,64,4096]{3,2,0,1:T(8,128)(2,1)S(1)} %copy-done.9, f32[8,1,64,512]{3,2,0,1:T(8,128)S(1)} %fusion.26), kind=kOutput, calls=%fused_computation.36 | convolution fusion | flops 2149056512 | bytes 9961472 | tf_op jit(solution)/shard_map/sqid,qdf->sqif/dot_general | solution.py:144
  222.9 35.2 %all-gather.9.cloned.1.call-done = bf16[8,1,64,2048]{3,2,0,1:T(8,128)(2,1)} async-done(((bf16[8,1,64,512]{3,2,0,1:T(8,128)(2,1)}), bf16[8,1,64,2048]{3,2,0,1:T(8,128)(2,1)}) %all-gather.9.cloned.1.call-update) | async-done | bytes 2097168 | tf_op jit(solution)/shard_map/all_gather | solution.py:148
  258.1 6.1 %fusion.21 = bf16[8,1,64,1024]{3,2,1,0:T(8,128)(2,1)} fusion(bf16[1,2048,1024]{2,1,0:T(8,128)(2,1)} %param.35, bf16[8,1,64,2048]{3,2,0,1:T(8,128)(2,1)} %all-gather.9.cloned.1.call-done), kind=kOutput, calls=%fused_computation.32 | convolution fusion | flops 2148007936 | bytes 7340032 | tf_op jit(solution)/shard_map/sqif,qfe->sqie/dot_general | solution.py:146
  264.3 4.6 %all-to-all-start.1 = ((bf16[8,1,64,1024]{3,2,1,0:T(8,128)(2,1)}), bf16[8,1,64,1024]{3,2,1,0:T(8,128)(2,1)S(1)}, u32[]{:S(2)}, u32[]{:S(2)}) async-start(bf16[8,1,64,1024]{3,2,1,0:T(8,128)(2,1)} %fusion.21), calls=%async_computation.1 | async-start | bytes 2097152 | tf_op jit(solution)/shard_map/all_to_all | solution.py:221
  268.9 26.5 %all-to-all-done.1 = bf16[8,1,64,1024]{3,2,1,0:T(8,128)(2,1)S(1)} async-done(((bf16[8,1,64,1024]{3,2,1,0:T(8,128)(2,1)}), bf16[8,1,64,1024]{3,2,1,0:T(8,128)(2,1)S(1)}, u32[]{:S(2)}, u32[]{:S(2)}) %all-to-all-start.1) | async-done | bytes 1048608 | tf_op jit(solution)/shard_map/all_to_all | solution.py:221
  295.4 0.4 fusion.47
  295.8 1.1 fusion.48
  (61 shorter events, 1.6 us)
Async XLA Ops:
  6.5 64.0 %copy-start.2 = (s32[128]{0:T(128)S(1)}, s32[128]{0:T(128)}, u32[]{:S(2)}) copy-start(s32[128]{0:T(128)} %param.26) | copy-start | bytes 1540
  6.5 64.1 %copy-start.3 = (f32[128,4]{0,1:T(4,128)S(1)}, f32[128,4]{0,1:T(4,128)}, u32[]{:S(2)}) copy-start(f32[128,4]{0,1:T(4,128)} %param.23) | copy-start | bytes 6148
  6.5 51.1 %copy-start = (bf16[128,512]{1,0:T(8,128)(2,1)S(1)}, bf16[128,512]{1,0:T(8,128)(2,1)}, u32[]{:S(2)}) copy-start(bf16[128,512]{1,0:T(8,128)(2,1)} %param.20) | copy-start | bytes 393220
  6.5 63.9 %copy-start.4 = (s32[128,2]{0,1:T(2,128)S(1)}, s32[128,2]{0,1:T(2,128)}, u32[]{:S(2)}) copy-start(s32[128,2]{0,1:T(2,128)} %param.31) | copy-start | bytes 3076
  6.5 31.4 %copy-start.6 = (bf16[1024]{0:T(1024)(128)(2,1)S(1)}, bf16[1024]{0:T(1024)(128)(2,1)}, u32[]{:S(2)}) copy-start(bf16[1024]{0:T(1024)(128)(2,1)} %param.30) | copy-start | bytes 6148
  6.5 64.3 %all-gather.11.cloned.1.call-start = ((), (), s32[]{:S(2)}) async-start(), calls=%async_computation.4 | async-start | bytes 2359296 | tf_op jit(solution)/shard_map/all_gather | solution.py:16
  20.6 193.2 %all-gather.7.cloned.1.call-start = ((), (), s32[]{:S(2)}) async-start(), calls=%async_computation.2 | async-start | bytes 5242880 | tf_op jit(solution)/shard_map/all_gather | solution.py:214
  57.7 15.3 %copy-start.5 = (f32[512]{0:T(512)S(1)}, f32[512]{0:T(512)}, u32[]{:S(2)}) copy-start(f32[512]{0:T(512)} %param.27) | copy-start | bytes 6148
  70.9 11.8 %copy-start.1 = (bf16[128,1024]{1,0:T(8,128)(2,1)S(1)}, bf16[128,1024]{1,0:T(8,128)(2,1)}, u32[]{:S(2)}) copy-start(bf16[128,1024]{1,0:T(8,128)(2,1)} %param.28) | copy-start | bytes 786436
  163.1 95.1 %all-gather.9.cloned.1.call-start = ((), (), s32[]{:S(2)}) async-start(), calls=%async_computation.3 | async-start | bytes 2621440 | tf_op jit(solution)/shard_map/all_gather | solution.py:148
  213.7 5.9 %copy-start.8 = (bf16[1,4096,512]{2,1,0:T(8,128)(2,1)S(1)}, bf16[1,4096,512]{2,1,0:T(8,128)(2,1)}, u32[]{:S(2)}) copy-start(bf16[1,4096,512]{2,1,0:T(8,128)(2,1)} %param.34) | copy-start | bytes 12582916
  213.7 5.9 %copy-start.9 = (bf16[8,1,64,4096]{3,2,0,1:T(8,128)(2,1)S(1)}, bf16[8,1,64,4096]{3,2,0,1:T(8,128)(2,1)}, u32[]{:S(2)}) copy-start(bf16[8,1,64,4096]{3,2,0,1:T(8,128)(2,1)} %all-gather.7.cloned.1.call-done) | copy-start | bytes 12582916
  222.9 46.0 %copy-start.7 = (f32[128,2]{0,1:T(2,128)S(1)}, f32[128,2]{0,1:T(2,128)}, u32[]{:S(2)}) copy-start(f32[128,2]{0,1:T(2,128)} %param.32) | copy-start | bytes 3076
  264.3 31.2 %all-to-all-start.1 = ((bf16[8,1,64,1024]{3,2,1,0:T(8,128)(2,1)}), bf16[8,1,64,1024]{3,2,1,0:T(8,128)(2,1)S(1)}, u32[]{:S(2)}, u32[]{:S(2)}) async-start(bf16[8,1,64,1024]{3,2,1,0:T(8,128)(2,1)} %fusion.21), calls=%async_computation.1 | async-start | bytes 2097152 | tf_op jit(solution)/shard_map/all_to_all | solution.py:221
Sparse Core Ops, SparseCore 0:
  20.7 31.9 all-gather.10
  163.2 50.5 all-gather.6
  223.1 35.0 all-gather.8
where the time goes:
time: 304 us; the launch traced here: 303 us
  blocking collectives  129 us (42%)
  waiting for transfers between devices  112 us (37%)
  matrix products  22.8 us (8%)
  between operations  14.1 us (5%)
  local copies, waits for them, and re-layouts  10.6 us (3%)
  other arithmetic  9.33 us (3%)
  starting transfers between devices  4.73 us (2%)
    all_to_all x1, blocking collectives, per_device(): lax.all_to_all(packed, 'sp', split_axis=0, concat_axis=0, tiled=True)  67.8 us
    all_gather x1, waiting for transfers between devices, per_device(): lax.all_gather(lax.all_to_all(packed, 'sp', split_axis=0, concat_axis=0,...  50.6 us
    all_gather x1, waiting for transfers between devices, expert_work(): lax.all_gather(hidden, 'tp', axis=3, tiled=True)  35.2 us
    all_gather x3, blocking collectives, prefix_2(): gathered = jax.tree.map(lambda a: lax.all_gather(a, axis), part)  32.4 us
    all_to_all x1, waiting for transfers between devices, per_device(): lax.all_to_all(served, 'sp', split_axis=0, concat_axis=0, tiled=True)  26.5 us
    unnamed x1, blocking collectives  10.6 us
    all_gather x1, blocking collectives, per_device(): lax.all_gather(memory_cell_output, 'tp', axis=1, tiled=True)  9.63 us
    psum x1, blocking collectives, per_device(): squares = lax.psum(jnp.sum(rows_f * rows_f, axis=1), 'tp')  8.98 us
  transfers between devices with their start and end apart: 4, of which 3 were waited for; matrix products, arithmetic and copies ran while one was open for 2% of the time, Pallas kernels for 0%

commit v1 on v0

--- a/solution.py
+++ b/solution.py
@@ -143,12 +143,24 @@
     )
     upward = jnp.einsum("sqid,qdf->sqif", row_block, up_weight, preferred_element_type=jnp.float32)
     hidden = (jax.nn.silu(gate_act) * upward).astype(jnp.bfloat16)
-    result = jnp.einsum(
-        "sqif,qfe->sqie",
-        lax.all_gather(hidden, "tp", axis=3, tiled=True),
-        down_weight,
-        preferred_element_type=jnp.float32,
-    )
+    outcome_arr = lax.axis_size("tp")
+    even, inter, seen_now = (outcome_arr, lax.axis_index("tp"), hidden.shape[3])
+    line_up = []
+    for nth in [*range(even)]:
+        line_up.append((nth, (nth + 1) % even))
+    kept_arr, result = (hidden, None)
+    for ix in [*range(even)]:
+        main = lax.ppermute(kept_arr, "tp", line_up) if ix < even - 1 else None
+        e_next = jnp.einsum(
+            "sqif,qfe->sqie",
+            kept_arr,
+            lax.dynamic_slice_in_dim(
+                down_weight, (inter - ix) % even * seen_now, kept_arr.shape[3], axis=1
+            ),
+            preferred_element_type=jnp.float32,
+        )
+        result = e_next if result is None else result + e_next
+        kept_arr = main
     return result.astype(jnp.bfloat16)
 
 

time: 304 us -> 303 us (level)
    all_gather x1 -> x0, waiting for transfers between devices: 35.2 us -> none  [expert_work(): lax.all_gather(hidden, 'tp', axis=3, tiled=True)]
    ppermute x0 -> x3, waiting for transfers between devices: none -> 35 us  [expert_work(): main = lax.ppermute(kept_arr, 'tp', line_up) if ix < even - 1 else None]
    dot_general x1 -> x4, matrix products: 6.14 us -> 5.29 us  [expert_work(): jnp.einsum('sqif,qfe->sqie', kept_arr, lax.dynamic_slice_in_dim(down_weig...]
    unnamed x28 -> x30, local copies, waits for them, and re-layouts: 6.26 us -> 6.26 us
  transfers between devices with their start and end apart: 4 -> 6, of which waited for: 3 -> 5; matrix products, arithmetic and copies ran while one was open for 2% -> 4% of each run, Pallas kernels for 0% -> 0%
where the time goes in v1:
time: 303 us; the launch traced here: 302 us
  blocking collectives  127 us (42%)
  waiting for transfers between devices  112 us (37%)
  matrix products  21.1 us (7%)
  between operations  14.4 us (5%)
  local copies, waits for them, and re-layouts  10.6 us (3%)
  other arithmetic  9.33 us (3%)
  starting transfers between devices  6.77 us (2%)
    all_to_all x1, blocking collectives, per_device(): lax.all_to_all(packed, 'sp', split_axis=0, concat_axis=0, tiled=True)  65.6 us
    all_gather x1, waiting for transfers between devices, per_device(): lax.all_gather(lax.all_to_all(packed, 'sp', split_axis=0, concat_axis=0,...  50.7 us
    ppermute x3, waiting for transfers between devices, expert_work(): main = lax.ppermute(kept_arr, 'tp', line_up) if ix < even - 1 else None  35 us
    all_gather x3, blocking collectives, prefix_2(): gathered = jax.tree.map(lambda a: lax.all_gather(a, axis), part)  32.4 us
    all_to_all x1, waiting for transfers between devices, per_device(): lax.all_to_all(served, 'sp', split_axis=0, concat_axis=0, tiled=True)  26.5 us
    unnamed x1, blocking collectives  10.6 us
    all_gather x1, blocking collectives, per_device(): lax.all_gather(memory_cell_output, 'tp', axis=1, tiled=True)  9.65 us
    psum x1, blocking collectives, per_device(): squares = lax.psum(jnp.sum(rows_f * rows_f, axis=1), 'tp')  8.96 us
  transfers between devices with their start and end apart: 6, of which 5 were waited for; matrix products, arithmetic and copies ran while one was open for 4% of the time, Pallas kernels for 0%

profile of v1, /device:TPU:0, one launch (start us, length us, event | category | flops | bytes accessed | tf_op | source)
XLA Modules:
  0.0 301.8 jit_solution(4216754828797818057)
XLA Ops:
  6.6 0.8 fusion.77
  7.7 1.5 fusion.88
  9.2 1.3 dynamic-slice
  10.5 2.0 slice_dynamic-update-slice_fusion
  12.5 1.3 broadcast_compare_fusion.1
  13.8 0.7 fusion.85
  14.5 0.6 iota_compare_fusion.10
  15.7 0.9 select_reduce_fusion
  16.7 0.8 select_multiply_fusion
  17.4 1.0 copy.177
  18.5 1.0 copy.183
  19.5 1.1 fusion.64
  20.7 0.7 dynamic-update-slice.1
  21.4 1.4 slice_dynamic-update-slice_fusion.1
  22.8 10.6 %all-reduce.3 = (s32[8]{0:T(128)S(1)}, s32[8]{0:T(128)S(1)}, s32[8]{0:T(128)S(1)}) all-reduce(s32[8]{0:T(128)S(1)} %slice_dynamic-update-slice_fusion.1, s32[8]{0:T(128)S(1)} %dynamic-update-slice.1, s32[8]{0:T(128)S(1)} %get-tuple-element.244), channel_id=1, replica_groups=mesh['sp'=8,'tp'=4] {'sp'}, use_global_device_ids=true, to_apply=%add | all-reduce | flops 24 | bytes 192
  33.4 0.8 copy.162
  34.7 1.0 copy.176
  35.7 1.0 add_divide_fusion
  36.8 0.6 reduce-window.18
  37.4 0.2 slice_reduce_fusion
  38.0 9.5 %all-gather.2 = f32[8,1,4]{2,1,0:T(1,128)S(1)} all-gather(f32[1,1,4]{2,1,0:T(1,128)S(1)} %bitcast.281), channel_id=1, replica_groups=mesh['sp'=8,'tp'=4] {'sp'}, dimensions={0}, use_global_device_ids=true | all-gather | bytes 144 | tf_op jit(solution)/shard_map/all_gather | solution.py:16
  47.5 10.1 %all-gather.1 = f32[8,1,4]{2,1,0:T(1,128)S(1)} all-gather(f32[1,1,4]{2,1,0:T(1,128)S(1)} %get-tuple-element.235), channel_id=1, replica_groups=mesh['sp'=8,'tp'=4] {'sp'}, dimensions={0}, use_global_device_ids=true | all-gather | bytes 144 | tf_op jit(solution)/shard_map/all_gather | solution.py:16
  57.7 12.8 %all_gather.50 = f32[8,4,128]{2,1,0:T(4,128)S(1)} all-gather(f32[1,4,128]{2,1,0:T(4,128)S(1)} %bitcast.278), channel_id=1, replica_groups=mesh['sp'=8,'tp'=4] {'sp'}, dimensions={0}, use_global_device_ids=true | all-gather | bytes 18432 | tf_op jit(solution)/shard_map/all_gather | solution.py:16
  70.6 0.2 fusion.66
  71.6 0.4 fusion.89
  72.0 0.3 convolution_bitcast_fusion.1
  72.5 0.4 multiply_reduce_fusion.1
  73.1 9.6 %all_gather.51 = bf16[128,2048]{0,1:T(8,128)(2,1)S(1)} all-gather(bf16[128,512]{0,1:T(8,128)(2,1)S(1)} %bitcast.265), channel_id=1, replica_groups=mesh['sp'=8,'tp'=4] {'tp'}, dimensions={1}, use_global_device_ids=true | all-gather | bytes 655360 | tf_op jit(solution)/shard_map/all_gather | solution.py:203
  82.7 3.0 %multiply_reduce_fusion = (f32[128]{0:T(128)S(1)}, f32[128,1024]{1,0:T(8,128)S(1)}) fusion(bf16[128,2048]{0,1:T(8,128)(2,1)S(1)} %all_gather.51, bf16[2048,1024]{1,0:T(8,128)(2,1)} %param.29, bf16[128,1024]{1,0:T(8,128)(2,1)S(1)} %copy-done.1), kind=kOutput, calls=%fused_computation.68 | convolution fusion | flops 537657216 | bytes 5505536 | tf_op jit(solution)/shard_map/dot_general | solution.py:202
  85.8 9.0 %psum.7 = f32[128]{0:T(128)S(1)} all-reduce(f32[128]{0:T(128)S(1)} %get-tuple-element.252), channel_id=1, replica_groups=mesh['sp'=8,'tp'=4] {'tp'}, use_global_device_ids=true, to_apply=%region_17.18 | all-reduce | flops 128 | bytes 1024 | tf_op jit(solution)/shard_map/psum | solution.py:221
  94.7 0.5 convolution_convert_fusion
  95.3 65.6 %all_to_all.10 = bf16[8,1,64,1024]{3,2,1,0:T(8,128)(2,1)} all-to-all(bf16[8,1,64,1024]{3,2,1,0:T(8,128)(2,1)S(1)} %bitcast.258), channel_id=1, replica_groups=mesh['sp'=8,'tp'=4] {'sp'}, dimensions={0} | all-to-all | bytes 2097152 | tf_op jit(solution)/shard_map/all_to_all | solution.py:227
  160.9 50.7 %all-gather.6.cloned.1.call-done = bf16[8,1,64,4096]{3,2,0,1:T(8,128)(2,1)} async-done(((bf16[8,1,64,1024]{3,2,0,1:T(8,128)(2,1)}), bf16[8,1,64,4096]{3,2,0,1:T(8,128)(2,1)}) %all-gather.6.cloned.1.call-update) | async-done | bytes 4194320 | tf_op jit(solution)/shard_map/all_gather | solution.py:226
  211.5 5.9 %fusion.14 = f32[8,1,64,512]{3,2,0,1:T(8,128)S(1)} fusion(bf16[1,4096,512]{2,1,0:T(8,128)(2,1)} %param.33, bf16[8,1,64,4096]{3,2,0,1:T(8,128)(2,1)} %all-gather.6.cloned.1.call-done), kind=kOutput, calls=%fused_computation.30 | convolution fusion | flops 2147483648 | bytes 9437184 | tf_op jit(solution)/shard_map/sqid,qdf->sqif/dot_general | solution.py:141
  217.5 2.4 fusion.29
  219.9 1.5 collective-permute-start
  221.4 12.9 %collective-permute-done = bf16[8,1,64,512]{3,2,0,1:T(8,128)(2,1)S(1)} collective-permute-done((bf16[8,1,64,512]{3,2,0,1:T(8,128)(2,1)S(1)}, bf16[8,1,64,512]{3,2,0,1:T(8,128)(2,1)S(1)}, u32[]{:S(2)}, u32[]{:S(2)}) %collective-permute-start) | collective-permute-done | bytes 524320 | tf_op jit(solution)/shard_map/ppermute | solution.py:153
  234.4 0.6 collective-permute-start.1
  234.9 2.1 fusion.50
  237.0 10.9 %collective-permute-done.1 = bf16[8,1,64,512]{3,2,0,1:T(8,128)(2,1)S(1)} collective-permute-done((bf16[8,1,64,512]{3,2,0,1:T(8,128)(2,1)S(1)}, bf16[8,1,64,512]{3,2,0,1:T(8,128)(2,1)S(1)}, u32[]{:S(2)}, u32[]{:S(2)}) %collective-permute-start.1) | collective-permute-done | bytes 524320 | tf_op jit(solution)/shard_map/ppermute | solution.py:153
  247.9 0.7 fusion.48
  248.6 0.7 fusion.46
  249.4 11.2 %collective-permute-done.2 = bf16[8,1,64,512]{3,2,0,1:T(8,128)(2,1)S(1)} collective-permute-done((bf16[8,1,64,512]{3,2,0,1:T(8,128)(2,1)S(1)}, bf16[8,1,64,512]{3,2,0,1:T(8,128)(2,1)S(1)}, u32[]{:S(2)}, u32[]{:S(2)}) %collective-permute-start.2) | collective-permute-done | bytes 524320 | tf_op jit(solution)/shard_map/ppermute | solution.py:153
  260.6 1.8 fusion.13
  262.4 4.6 %all-to-all-start.1 = ((bf16[8,1,64,1024]{3,2,1,0:T(8,128)(2,1)}), bf16[8,1,64,1024]{3,2,1,0:T(8,128)(2,1)S(1)}, u32[]{:S(2)}, u32[]{:S(2)}) async-start(bf16[8,1,64,1024]{3,2,1,0:T(8,128)(2,1)} %fusion.13), calls=%async_computation.1 | async-start | bytes 2097152 | tf_op jit(solution)/shard_map/all_to_all | solution.py:233
  267.0 26.5 %all-to-all-done.1 = bf16[8,1,64,1024]{3,2,1,0:T(8,128)(2,1)S(1)} async-done(((bf16[8,1,64,1024]{3,2,1,0:T(8,128)(2,1)}), bf16[8,1,64,1024]{3,2,1,0:T(8,128)(2,1)S(1)}, u32[]{:S(2)}, u32[]{:S(2)}) %all-to-all-start.1) | async-done | bytes 1048608 | tf_op jit(solution)/shard_map/all_to_all | solution.py:233
  293.5 0.4 fusion.35
  293.9 1.1 fusion.36
  (69 shorter events, 2.7 us)
Async XLA Ops:
  6.5 64.0 %copy-start.3 = (s32[128]{0:T(128)S(1)}, s32[128]{0:T(128)}, u32[]{:S(2)}) copy-start(s32[128]{0:T(128)} %param.26) | copy-start | bytes 1540
  6.5 64.1 %copy-start.4 = (f32[128,4]{0,1:T(4,128)S(1)}, f32[128,4]{0,1:T(4,128)}, u32[]{:S(2)}) copy-start(f32[128,4]{0,1:T(4,128)} %param.23) | copy-start | bytes 6148
  6.5 51.1 %copy-start = (bf16[128,512]{1,0:T(8,128)(2,1)S(1)}, bf16[128,512]{1,0:T(8,128)(2,1)}, u32[]{:S(2)}) copy-start(bf16[128,512]{1,0:T(8,128)(2,1)} %param.20) | copy-start | bytes 393220
  6.5 63.9 %copy-start.5 = (s32[128,2]{0,1:T(2,128)S(1)}, s32[128,2]{0,1:T(2,128)}, u32[]{:S(2)}) copy-start(s32[128,2]{0,1:T(2,128)} %param.31) | copy-start | bytes 3076
  6.5 31.4 %copy-start.7 = (bf16[1024]{0:T(1024)(128)(2,1)S(1)}, bf16[1024]{0:T(1024)(128)(2,1)}, u32[]{:S(2)}) copy-start(bf16[1024]{0:T(1024)(128)(2,1)} %param.30) | copy-start | bytes 6148
  6.5 64.3 %all-gather.8.cloned.1.call-start = ((), (), s32[]{:S(2)}) async-start(), calls=%async_computation.3 | async-start | bytes 2359296 | tf_op jit(solution)/shard_map/all_gather | solution.py:16
  20.6 190.9 %all-gather.6.cloned.1.call-start = ((), (), s32[]{:S(2)}) async-start(), calls=%async_computation.2 | async-start | bytes 5242880 | tf_op jit(solution)/shard_map/all_gather | solution.py:226
  57.7 15.3 %copy-start.6 = (f32[512]{0:T(512)S(1)}, f32[512]{0:T(512)}, u32[]{:S(2)}) copy-start(f32[512]{0:T(512)} %param.27) | copy-start | bytes 6148
  70.9 11.8 %copy-start.1 = (bf16[128,1024]{1,0:T(8,128)(2,1)S(1)}, bf16[128,1024]{1,0:T(8,128)(2,1)}, u32[]{:S(2)}) copy-start(bf16[128,1024]{1,0:T(8,128)(2,1)} %param.28) | copy-start | bytes 786436
  211.5 5.9 %copy-start.9 = (bf16[1,4096,512]{2,1,0:T(8,128)(2,1)S(1)}, bf16[1,4096,512]{2,1,0:T(8,128)(2,1)}, u32[]{:S(2)}) copy-start(bf16[1,4096,512]{2,1,0:T(8,128)(2,1)} %param.34) | copy-start | bytes 12582916
  211.5 5.9 %copy-start.10 = (bf16[8,1,64,4096]{3,2,0,1:T(8,128)(2,1)S(1)}, bf16[8,1,64,4096]{3,2,0,1:T(8,128)(2,1)}, u32[]{:S(2)}) copy-start(bf16[8,1,64,4096]{3,2,0,1:T(8,128)(2,1)} %all-gather.6.cloned.1.call-done) | copy-start | bytes 12582916
  219.9 14.5 %collective-permute-start = (bf16[8,1,64,512]{3,2,0,1:T(8,128)(2,1)S(1)}, bf16[8,1,64,512]{3,2,0,1:T(8,128)(2,1)S(1)}, u32[]{:S(2)}, u32[]{:S(2)}) collective-permute-start(bf16[8,1,64,512]{3,2,0,1:T(8,128)(2,1)S(1)} %fusion.29), channel_id=1, source_target_pairs={{0,1},{1,2},{2,3},{3,0},{4,5},{5,6},{6,7},{7,4},{8,9},{9,10},{10,1... | collective-permute-start | bytes 1572872 | tf_op jit(solution)/shard_map/ppermute | solution.py:153
  234.4 13.5 %collective-permute-start.1 = (bf16[8,1,64,512]{3,2,0,1:T(8,128)(2,1)S(1)}, bf16[8,1,64,512]{3,2,0,1:T(8,128)(2,1)S(1)}, u32[]{:S(2)}, u32[]{:S(2)}) collective-permute-start(bf16[8,1,64,512]{3,2,0,1:T(8,128)(2,1)S(1)} %collective-permute-done), channel_id=1, source_target_pairs={{0,1},{1,2},{2,3},{3,0},{4,5},{5,6},{6,7},{7,4},{8,9},{9,10},{10,1... | collective-permute-start | bytes 1572872 | tf_op jit(solution)/shard_map/ppermute | solution.py:153
  234.9 13.0 %copy-start.2 = (bf16[1,2048,1024]{2,1,0:T(8,128)(2,1)S(1)}, bf16[1,2048,1024]{2,1,0:T(8,128)(2,1)}, u32[]{:S(2)}) copy-start(bf16[1,2048,1024]{2,1,0:T(8,128)(2,1)} %param.35) | copy-start | bytes 12582916
  247.9 12.7 %collective-permute-start.2 = (bf16[8,1,64,512]{3,2,0,1:T(8,128)(2,1)S(1)}, bf16[8,1,64,512]{3,2,0,1:T(8,128)(2,1)S(1)}, u32[]{:S(2)}, u32[]{:S(2)}) collective-permute-start(bf16[8,1,64,512]{3,2,0,1:T(8,128)(2,1)S(1)} %collective-permute-done.1), channel_id=1, source_target_pairs={{0,1},{1,2},{2,3},{3,0},{4,5},{5,6},{6,7},{7,4},{8,9},{9,10},{10,1... | collective-permute-start | bytes 1572872 | tf_op jit(solution)/shard_map/ppermute | solution.py:153
  249.4 17.6 %copy-start.8 = (f32[128,2]{0,1:T(2,128)S(1)}, f32[128,2]{0,1:T(2,128)}, u32[]{:S(2)}) copy-start(f32[128,2]{0,1:T(2,128)} %param.32) | copy-start | bytes 3076
  262.4 31.2 %all-to-all-start.1 = ((bf16[8,1,64,1024]{3,2,1,0:T(8,128)(2,1)}), bf16[8,1,64,1024]{3,2,1,0:T(8,128)(2,1)S(1)}, u32[]{:S(2)}, u32[]{:S(2)}) async-start(bf16[8,1,64,1024]{3,2,1,0:T(8,128)(2,1)} %fusion.13), calls=%async_computation.1 | async-start | bytes 2097152 | tf_op jit(solution)/shard_map/all_to_all | solution.py:233
Sparse Core Ops, SparseCore 0:
  20.7 31.9 all-gather.7
  161.0 50.5 all-gather.5
